TPU v7x, 32 devices: a whole 2x2x4 slice. The times are simulated.
32 devices in a mesh: ep: 16 (over z, x, core), tp: 2 (over y).
Axes of the slice: x: 2, y: 2, z: 4, core: 2. Of those that a mesh axis runs over, the one named last changes fastest.
Arguments:
- residual_in: bfloat16 [240, 1536], P('ep'), may hold values from -6 to 6
- rec_state: bfloat16 [240, 12, 128, 128], P('ep', 'tp'), may hold values from -6 to 6
- mix_gain: float32 [1536], replicated, may hold values from 0.1 to 1.9
- w_query: bfloat16 [1536, 1536], P('tp', 'ep'), may hold values from -0.15625 to 0.15625
- w_forget: bfloat16 [1536, 1536], P('tp', 'ep'), may hold values from -0.15625 to 0.15625
- w_input: bfloat16 [1536, 1536], P('tp', 'ep'), may hold values from -0.15625 to 0.15625
- w_gate: bfloat16 [1536, 1536], P('tp', 'ep'), may hold values from -0.15625 to 0.15625
- lower_bound: float32 [1536], P('tp'), may hold values from 0 to 0.9
- head_gain: float32 [128], replicated, may hold values from 0.1 to 1.9
- w_out: bfloat16 [1536, 1536], P('tp', 'ep'), may hold values from -0.15625 to 0.15625
- ffn_gain: float32 [1536], replicated, may hold values from 0.1 to 1.9
- route_ids: int32 [240, 6], P('ep'), may hold values from 0 to 15, all different within a row; in each aligned block of 15 rows (0 to 14, 15 to 29, ...) at most 6 rows name the same one
- route_weight: float32 [240, 6], P('ep'), may hold values from 0.2 to 1
- expert_gate: bfloat16 [16, 1536, 512], P('ep', None, 'tp'), may hold values from -0.15625 to 0.15625
- expert_up: bfloat16 [16, 1536, 512], P('ep', None, 'tp'), may hold values from -0.15625 to 0.15625
- expert_down: bfloat16 [16, 512, 1536], P('ep', 'tp'), may hold values from -0.25 to 0.25
Outputs:
- layer_out: bfloat16 [240, 1536], P('ep', 'tp')
- new_state: bfloat16 [240, 12, 128, 128], P('ep', 'tp')
Inputs may be any that keep to these rules, and one draw needn't show every extreme that they name: `route_ids`: each row names 6 different experts. Among the rows of one device no expert is named more than 6 times, and in every draw some device names some expert exactly 6 times.
All inputs are finite; a program needn't handle non-finite values.
Results may differ from a plain program's by a relative error of at most 0.016.
Values may be sent and summed in bfloat16 or wider, within the bound.
No kernel may reach another device: no remote copies, remote signals or barrier semaphores. Data moves between devices by JAX's collectives and lax.ppermute only.
A program may use at most 64 MiB of HBM per device.

v0:
```python
import jax
import jax.numpy as jnp
from jax import lax
from jax.sharding import PartitionSpec as P

rms_eps = 1e-06


def rms_scale(values, gain):
    return values * lax.rsqrt(jnp.mean(values * values, axis=-1, keepdims=True) + rms_eps) * gain


def rounded(values):
    return lax.optimization_barrier(values.astype(jnp.bfloat16)).astype(jnp.float32)


def recurrence(lower_bound, head_gain, state_block, query_raw, forget_raw, input_raw, gate_raw):
    seq_count = state_block.shape[0]
    heads_local = state_block.shape[1]
    head_size = state_block.shape[2]
    head_shape = (seq_count, heads_local, head_size)
    forget = lower_bound + (1.0 - lower_bound) * jax.nn.sigmoid(forget_raw)
    query_act = jax.nn.silu(query_raw).reshape(head_shape)
    key_act = (1.0 - forget).reshape(head_shape)
    forget_heads = forget.reshape(head_shape)
    value_act = input_raw.reshape(head_shape)
    state_next = (
        forget_heads[:, :, :, None] * state_block.astype(jnp.float32)
        + key_act[:, :, :, None] * value_act[:, :, None, :]
    )
    readout = jnp.einsum("shk,shkv->shv", query_act, state_next, precision=lax.Precision.HIGHEST)
    gate_heads = jax.nn.silu(gate_raw).reshape(head_shape)
    heads_out = rms_scale(readout, head_gain) * gate_heads
    return (
        state_next.astype(jnp.bfloat16),
        heads_out.reshape(seq_count, heads_local * head_size).astype(jnp.bfloat16),
    )


def shards(
    residual_in,
    rec_state,
    mix_gain,
    w_query,
    w_forget,
    w_input,
    w_gate,
    lower_bound,
    head_gain,
    w_out,
    ffn_gain,
    route_ids,
    route_weight,
    expert_gate,
    expert_up,
    expert_down,
):
    tp_count = lax.axis_size("tp")
    tp_rank = lax.axis_index("tp")
    ep_count = lax.axis_size("ep")
    seq_count = residual_in.shape[0]
    model_width = residual_in.shape[1]
    quarter = model_width // tp_count
    residual = residual_in.astype(jnp.float32)
    normed = rms_scale(residual, mix_gain).astype(jnp.bfloat16)
    own_rows = lax.dynamic_slice_in_dim(normed, tp_rank * quarter, quarter, 1)
    rows_piece = lax.all_gather(own_rows, "ep", axis=0, tiled=True)
    partial_proj = jnp.stack(
        [
            jnp.dot(rows_piece, weight, preferred_element_type=jnp.float32)
            for weight in (w_query, w_forget, w_input, w_gate)
        ],
        axis=1,
    )
    arrived = lax.all_to_all(partial_proj, "ep", split_axis=0, concat_axis=2, tiled=True)
    summed = lax.psum_scatter(arrived, "tp", scatter_dimension=2, tiled=True)
    projected = rounded(summed)
    new_state, heads_out = recurrence(
        lower_bound,
        head_gain,
        rec_state,
        projected[:, 0],
        projected[:, 1],
        projected[:, 2],
        projected[:, 3],
    )
    partial_mix = jnp.dot(
        lax.all_gather(heads_out, "ep", axis=0, tiled=True),
        w_out,
        preferred_element_type=jnp.float32,
    )
    mixed_home = lax.all_to_all(
        partial_mix.astype(jnp.bfloat16), "ep", split_axis=0, concat_axis=1, tiled=True
    ).astype(partial_mix.dtype)
    mixed = lax.psum(mixed_home.astype(jnp.bfloat16), "tp").astype(jnp.float32)
    after_mix = rounded(residual + mixed)
    normed_ffn = rms_scale(after_mix, ffn_gain).astype(jnp.bfloat16)
    exp_dev = expert_gate.shape[0]
    experts_all = ep_count * exp_dev
    top_count = route_ids.shape[1]
    capacity = max(2, seq_count * top_count // experts_all + 1)
    flat_ids = route_ids.reshape(-1)
    onehot = (flat_ids[:, None] == jnp.arange(experts_all, dtype=jnp.int32)[None, :]).astype(
        jnp.int32
    )
    slot_rank = jnp.sum(jnp.cumsum(onehot, axis=0) * onehot, axis=1) - 1
    slot_index = flat_ids * capacity + slot_rank
    placer_int = (
        jnp.arange(experts_all * capacity, dtype=jnp.int32)[:, None] == slot_index[None, :]
    ).astype(jnp.int32)
    placer = jnp.sum(
        placer_int.reshape(experts_all * capacity, seq_count, top_count), axis=2
    ).astype(jnp.bfloat16)
    buffer = (
        jnp.dot(placer, normed_ffn, preferred_element_type=jnp.float32)
        .astype(jnp.bfloat16)
        .reshape(experts_all, capacity, model_width)
    )
    received = lax.all_to_all(buffer, "ep", split_axis=0, concat_axis=0, tiled=True)
    slot_count = received.shape[1]
    grouped = received.reshape(ep_count, exp_dev, slot_count, model_width)
    gate_part = jnp.einsum(
        "sjnd,jdf->sjnf", grouped, expert_gate, preferred_element_type=jnp.float32
    )
    up_part = jnp.einsum("sjnd,jdf->sjnf", grouped, expert_up, preferred_element_type=jnp.float32)
    hidden = (jax.nn.silu(gate_part) * up_part).astype(jnp.bfloat16)
    down_part = jnp.einsum(
        "sjnf,jfd->sjnd", hidden, expert_down, preferred_element_type=jnp.float32
    )
    summed_down = lax.psum_scatter(
        down_part.astype(jnp.bfloat16), "tp", scatter_dimension=3, tiled=True
    )
    returned = summed_down.reshape(experts_all, slot_count, quarter)
    gathered_back = lax.all_to_all(returned, "ep", split_axis=0, concat_axis=0, tiled=True)
    flat_back = gathered_back.reshape(experts_all * capacity, quarter)
    picked = (
        jnp.take(flat_back, slot_index, axis=0)
        .astype(jnp.float32)
        .reshape(seq_count, top_count, quarter)
    )
    expert_sum = jnp.sum(route_weight[:, :, None] * picked, axis=1)
    own_mix = lax.dynamic_slice_in_dim(after_mix, tp_rank * quarter, quarter, 1)
    layer_out = (own_mix + expert_sum).astype(jnp.bfloat16)
    return (layer_out, new_state)


def solution(mesh):
    in_specs = (
        P("ep", None),
        P("ep", "tp", None, None),
        P(),
        P("tp", "ep"),
        P("tp", "ep"),
        P("tp", "ep"),
        P("tp", "ep"),
        P("tp"),
        P(),
        P("tp", "ep"),
        P(),
        P("ep", None),
        P("ep", None),
        P("ep", None, "tp"),
        P("ep", None, "tp"),
        P("ep", "tp", None),
    )
    out_specs = (P("ep", "tp"), P("ep", "tp", None, None))
    return jax.shard_map(shards, mesh=mesh, in_specs=in_specs, out_specs=out_specs, check_vma=False)
```

profile of v0, /device:TPU:0, one launch (start us, length us, event | category | flops | bytes accessed | tf_op | source)
XLA Modules:
  0.0 206.5 jit_solution(8427857682327721564)
XLA Ops:
  7.2 0.0 copy-start
  7.2 0.9 convert_element_type.76
  8.1 0.9 multiply_reduce_fusion.2
  9.0 0.8 dynamic-slice
  9.8 0.1 fusion.36
  9.9 24.1 %all-gather = bf16[16,15,768]{2,1,0:T(8,128)(2,1)S(1)} all-gather(bf16[1,15,768]{2,1,0:T(8,128)(2,1)S(1)} %fusion.36), channel_id=1, replica_groups=mesh['ep'=16,'tp'=2] {'ep'}, dimensions={0}, use_global_device_ids=true | all-gather | bytes 391680 | tf_op jit(solution)/shard_map/all_gather | solution.py:67
  34.0 0.1 reshape.208
  34.1 1.2 convolution_bitcast_fusion.2
  35.3 1.2 convolution_bitcast_fusion.3
  36.5 1.2 convolution_bitcast_fusion.4
  37.7 1.2 convolution_bitcast_fusion.5
  38.9 1.0 copy.50
  39.9 3.6 %all-to-all-start = ((f32[240,4,96]{2,1,0:T(4,128)}), f32[240,4,96]{2,1,0:T(4,128)S(1)}, u32[]{:S(2)}, u32[]{:S(2)}) async-start(f32[240,4,96]{2,1,0:T(4,128)} %copy.50), calls=%async_computation | async-start | bytes 983040 | tf_op jit(solution)/shard_map/all_to_all | solution.py:75
  43.4 0.0 reduce-scatter.7.cloned.1.call-start
  43.5 0.1 copy.55
  43.6 0.1 reshape.191
  43.7 0.1 fusion.31
  43.8 0.1 reduce_window_sum.11
  43.9 13.2 %all-to-all-done = f32[240,4,96]{2,1,0:T(4,128)S(1)} async-done(((f32[240,4,96]{2,1,0:T(4,128)}), f32[240,4,96]{2,1,0:T(4,128)S(1)}, u32[]{:S(2)}, u32[]{:S(2)}) %all-to-all-start) | async-done | bytes 368672 | tf_op jit(solution)/shard_map/all_to_all | solution.py:75
  57.2 7.4 %copy.65 = f32[15,4,16,96]{1,0,3,2:T(8,128)} copy(f32[15,4,16,96]{3,1,0,2:T(4,128)S(1)} %bitcast.97) | data formatting | bytes 737280
  64.5 9.6 %reshape.217 = f32[1536,60]{1,0:T(8,128)} reshape(f32[1536,15,4]{2,1,0:T(8,128)} %bitcast.95) | data formatting | bytes 737280
  74.2 0.0 reduce-scatter.7.cloned.1.call-update
  74.2 0.2 select_reduce_fusion
  74.4 0.1 sub.25
  74.5 0.1 copy.57
  74.6 16.6 %reduce-scatter.7.cloned.1.call-done = f32[768,60]{1,0:T(8,128)} async-done(((f32[1536,60]{1,0:T(8,128)}), f32[768,60]{1,0:T(8,128)}) %reduce-scatter.7.cloned.1.call-update) | async-done | bytes 184336
  91.1 5.3 %reshape.218 = bf16[768,15,4]{2,1,0:T(8,128)(2,1)} reshape(f32[768,60]{1,0:T(8,128)} %reduce-scatter.7.cloned.1.call-done) | data formatting | bytes 276480
  96.4 4.4 %copy.64 = bf16[15,4,768]{2,1,0:T(4,128)(2,1)S(1)} copy(bf16[15,4,768]{1,0,2:T(8,128)(2,1)} %bitcast.96) | data formatting | bytes 184320
  100.9 0.6 slice_reduce_fusion
  101.5 0.0 copy-start.2
  101.6 8.9 %fusion.1 = f32[15,6,1,128]{3,2,1,0:T(1,128)S(1)} fusion(bf16[15,6,128,128]{3,2,1,0:T(8,128)(2,1)} %param.17, f32[15,6,128]{2,1,0:T(8,128)S(1)} %mul.167, f32[15,6,128]{2,1,0:T(8,128)S(1)} %get-tuple-element.8, f32[15,6,128]{2,1,0:T(8,128)S(1)} %get-tuple-element.9, f32[15,6,128,1]{2,1,0,3:T(8,128)S(1)} %multiply_bitcast_fusion), kind=kOutput, calls=%fused_computation.3 | convolution fusion | flops 23592960 | bytes 3179520 | tf_op jit(solution)/shard_map/shk,shkv->shv/dot_general | solution.py:31
  110.5 0.1 fusion.22
  110.6 0.1 fusion.25
  110.7 0.1 reshape.209
  110.8 22.4 %all-gather.1 = bf16[16,15,768]{2,1,0:T(8,128)(2,1)S(1)} all-gather(bf16[1,15,768]{2,1,0:T(8,128)(2,1)S(1)} %reshape.209), channel_id=1, replica_groups=mesh['ep'=16,'tp'=2] {'ep'}, dimensions={0}, use_global_device_ids=true | all-gather | bytes 391680 | tf_op jit(solution)/shard_map/all_gather | solution.py:88
  133.2 0.1 reshape.210
  133.3 1.2 convolution_convert_fusion.2
  134.5 0.1 copy.52
  134.6 0.7 all_to_all.37
  135.3 3.5 %all-to-all-start.1 = ((bf16[16,15,96]{2,1,0:T(8,128)(2,1)}), bf16[16,15,96]{2,1,0:T(8,128)(2,1)S(1)}, u32[]{:S(2)}, u32[]{:S(2)}) async-start(bf16[16,15,96]{2,1,0:T(8,128)(2,1)} %all_to_all.37), calls=%async_computation.1 | async-start | bytes 131072 | tf_op jit(solution)/shard_map/all_to_all | solution.py:92
  138.8 0.0 reduce-scatter.5.cloned.1.call-start
  138.8 0.1 convert_reduce_fusion
  138.9 6.7 %all-to-all-done.1 = bf16[16,15,96]{2,1,0:T(8,128)(2,1)S(1)} async-done(((bf16[16,15,96]{2,1,0:T(8,128)(2,1)}), bf16[16,15,96]{2,1,0:T(8,128)(2,1)S(1)}, u32[]{:S(2)}, u32[]{:S(2)}) %all-to-all-start.1) | async-done | bytes 46112 | tf_op jit(solution)/shard_map/all_to_all | solution.py:92
  145.7 0.1 all_to_all.40
  145.8 7.7 %psum.7 = bf16[15,1536]{1,0:T(8,128)(2,1)S(1)} all-reduce(bf16[15,1536]{1,0:T(8,128)(2,1)S(1)} %all_to_all.40), channel_id=1, replica_groups=mesh['ep'=16,'tp'=2] {'tp'}, use_global_device_ids=true, to_apply=%region_3.4 | all-reduce | flops 23040 | bytes 92160 | tf_op jit(solution)/shard_map/psum | solution.py:95
  153.5 0.1 multiply_reduce_fusion.1
  153.6 0.3 convolution_convert_fusion
  153.9 0.1 reshape.192
  154.0 14.8 %all_to_all.47 = bf16[16,6,1536]{2,1,0:T(8,128)(2,1)S(1)} all-to-all(bf16[16,6,1536]{2,1,0:T(8,128)(2,1)S(1)} %reshape.192), channel_id=1, replica_groups=mesh['ep'=16,'tp'=2] {'ep'}, dimensions={0} | all-to-all | bytes 589824 | tf_op jit(solution)/shard_map/all_to_all | solution.py:119
  168.8 0.3 convolution_bitcast_fusion.1
  169.1 1.4 fusion.5
  170.5 0.0 reduce-scatter.5.cloned.1.call-update
  170.5 0.1 mul.188
  170.6 0.1 copy.54
  170.7 11.0 %reduce-scatter.5.cloned.1.call-done = bf16[16,1,6,768]{3,0,2,1:T(8,128)(2,1)} async-done(((bf16[16,1,6,1536]{3,0,2,1:T(8,128)(2,1)}), bf16[16,1,6,768]{3,0,2,1:T(8,128)(2,1)}) %reduce-scatter.5.cloned.1.call-update) | async-done | bytes 147472 | tf_op jit(solution)/shard_map/reduce_scatter | solution.py:130
  181.7 1.6 copy.60
  183.3 5.6 %all-to-all-start.3 = ((bf16[16,6,768]{2,1,0:T(8,128)(2,1)}), bf16[16,6,768]{2,1,0:T(8,128)(2,1)S(1)}, u32[]{:S(2)}, u32[]{:S(2)}) async-start(bf16[16,6,768]{2,1,0:T(8,128)(2,1)} %copy.60), calls=%async_computation.4 | async-start | bytes 393216 | tf_op jit(solution)/shard_map/all_to_all | solution.py:134
  188.9 6.7 %fusion = bf16[15,6,128,128]{3,2,1,0:T(8,128)(2,1)} fusion(bf16[15,6,128,128]{3,2,1,0:T(8,128)(2,1)} %param.17, f32[15,6,128]{2,1,0:T(8,128)S(1)} %mul.167, f32[15,6,128]{2,1,0:T(8,128)S(1)} %get-tuple-element.8, f32[15,6,128]{2,1,0:T(8,128)S(1)} %get-tuple-element.9), kind=kLoop, calls=%fused_computation.2 | loop fusion | flops 7372800 | bytes 6036480 | tf_op jit(solution)/shard_map/convert_element_type | solution.py:35
  195.6 2.3 %all-to-all-done.3 = bf16[16,6,768]{2,1,0:T(8,128)(2,1)S(1)} async-done(((bf16[16,6,768]{2,1,0:T(8,128)(2,1)}), bf16[16,6,768]{2,1,0:T(8,128)(2,1)S(1)}, u32[]{:S(2)}, u32[]{:S(2)}) %all-to-all-start.3) | async-done | bytes 147488 | tf_op jit(solution)/shard_map/all_to_all | solution.py:134
  197.9 0.1 reshape.198
  197.9 0.8 gather_fusion
  198.7 0.1 gather.7
  198.8 0.2 multiply_reduce_fusion
  199.0 0.6 add_convert_fusion.1
  (36 shorter events, 0.3 us)
Async XLA Ops:
  7.2 161.9 %copy-start = (bf16[1,256,1536]{2,1,0:T(8,128)(2,1)S(1)}, bf16[1,256,1536]{2,1,0:T(8,128)(2,1)}, u32[]{:S(2)}) copy-start(bf16[1,256,1536]{2,1,0:T(8,128)(2,1)} %param.31) | copy-start | bytes 2359300
  7.2 36.3 %copy-start.6 = (s32[15,6]{0,1:T(8,128)S(1)}, s32[15,6]{0,1:T(8,128)}, u32[]{:S(2)}) copy-start(s32[15,6]{0,1:T(8,128)} %param.27) | copy-start | bytes 1084
  39.9 17.3 %all-to-all-start = ((f32[240,4,96]{2,1,0:T(4,128)}), f32[240,4,96]{2,1,0:T(4,128)S(1)}, u32[]{:S(2)}, u32[]{:S(2)}) async-start(f32[240,4,96]{2,1,0:T(4,128)} %copy.50), calls=%async_computation | async-start | bytes 983040 | tf_op jit(solution)/shard_map/all_to_all | solution.py:75
  43.4 47.7 %reduce-scatter.7.cloned.1.call-start = ((), (), s32[]{:S(2)}) async-start(), calls=%async_computation.7 | async-start | bytes 1179648
  64.5 10.0 %copy-start.4 = (f32[768]{0:T(1024)S(1)}, f32[768]{0:T(1024)}, u32[]{:S(2)}) copy-start(f32[768]{0:T(1024)} %param.23) | copy-start | bytes 9220
  96.4 14.2 %copy-start.8 = (f32[128]{0:T(128)S(1)}, f32[128]{0:T(128)}, u32[]{:S(2)}) copy-start(f32[128]{0:T(128)} %param.24) | copy-start | bytes 1540
  100.8 52.7 %copy-start.3 = (bf16[15,1536]{1,0:T(8,128)(2,1)S(1)}, bf16[15,1536]{1,0:T(8,128)(2,1)}, u32[]{:S(2)}) copy-start(bf16[15,1536]{1,0:T(8,128)(2,1)} %param.16) | copy-start | bytes 138244
  100.8 52.8 %copy-start.5 = (f32[1536]{0:T(1024)S(1)}, f32[1536]{0:T(1024)}, u32[]{:S(2)}) copy-start(f32[1536]{0:T(1024)} %param.26) | copy-start | bytes 18436
  101.4 67.4 %copy-start.1 = (bf16[1,1536,256]{2,1,0:T(8,128)(2,1)S(1)}, bf16[1,1536,256]{2,1,0:T(8,128)(2,1)}, u32[]{:S(2)}) copy-start(bf16[1,1536,256]{2,1,0:T(8,128)(2,1)} %param.29) | copy-start | bytes 2359300
  101.5 67.6 %copy-start.2 = (bf16[1,1536,256]{2,1,0:T(8,128)(2,1)S(1)}, bf16[1,1536,256]{2,1,0:T(8,128)(2,1)}, u32[]{:S(2)}) copy-start(bf16[1,1536,256]{2,1,0:T(8,128)(2,1)} %param.30) | copy-start | bytes 2359300
  101.5 69.0 %copy-start.7 = (f32[15,6]{0,1:T(8,128)S(1)}, f32[15,6]{0,1:T(8,128)}, u32[]{:S(2)}) copy-start(f32[15,6]{0,1:T(8,128)} %param.28) | copy-start | bytes 1084
  135.3 10.4 %all-to-all-start.1 = ((bf16[16,15,96]{2,1,0:T(8,128)(2,1)}), bf16[16,15,96]{2,1,0:T(8,128)(2,1)S(1)}, u32[]{:S(2)}, u32[]{:S(2)}) async-start(bf16[16,15,96]{2,1,0:T(8,128)(2,1)} %all_to_all.37), calls=%async_computation.1 | async-start | bytes 131072 | tf_op jit(solution)/shard_map/all_to_all | solution.py:92
  138.8 42.9 %reduce-scatter.5.cloned.1.call-start = ((), (), s32[]{:S(2)}) async-start(), calls=%async_computation.6 | async-start | bytes 442368 | tf_op jit(solution)/shard_map/reduce_scatter | solution.py:130
  183.3 14.6 %all-to-all-start.3 = ((bf16[16,6,768]{2,1,0:T(8,128)(2,1)}), bf16[16,6,768]{2,1,0:T(8,128)(2,1)S(1)}, u32[]{:S(2)}, u32[]{:S(2)}) async-start(bf16[16,6,768]{2,1,0:T(8,128)(2,1)} %copy.60), calls=%async_computation.4 | async-start | bytes 393216 | tf_op jit(solution)/shard_map/all_to_all | solution.py:134
Sparse Core Ops, SparseCore 0:
  74.3 16.7 reduce-scatter.6
  170.6 11.0 reduce-scatter.4
where the time goes:
time: 207 us; the launch traced here: 206 us
  blocking collectives  69 us (33%)
  waiting for transfers between devices  49.8 us (24%)
  local copies, waits for them, and re-layouts  32.9 us (16%)
  matrix products  16.7 us (8%)
  between operations  14.4 us (7%)
  starting transfers between devices  12.8 us (6%)
  other arithmetic  10.9 us (5%)
    unnamed x27, local copies, waits for them, and re-layouts  27.2 us
    all_gather x1, blocking collectives, shards(): rows_piece = lax.all_gather(own_rows, 'ep', axis=0, tiled=True)  24.1 us
    all_gather x1, blocking collectives, shards(): lax.all_gather(heads_out, 'ep', axis=0, tiled=True)  22.4 us
    unnamed x3, waiting for transfers between devices  16.6 us
    all_to_all x1, blocking collectives, shards(): lax.all_to_all(buffer, 'ep', split_axis=0, concat_axis=0, tiled=True)  14.8 us
    all_to_all x1, waiting for transfers between devices, shards(): lax.all_to_all(partial_proj, 'ep', split_axis=0, concat_axis=2, tiled=True)  13.2 us
    reduce_scatter x1, waiting for transfers between devices, shards(): lax.psum_scatter(down_part.astype(jnp.bfloat16), 'tp', scatter_dimension=...  11 us
    dot_general x1, matrix products, recurrence(): jnp.einsum('shk,shkv->shv', query_act, state_next, precision=lax.Precisio...  8.93 us
  transfers between devices with their start and end apart: 5, of which 5 were waited for; matrix products, arithmetic and copies ran while one was open for 4% of the time, Pallas kernels for 0%

commit v1 on v0

--- a/solution.py
+++ b/solution.py
@@ -72,7 +72,10 @@
         ],
         axis=1,
     )
-    arrived = lax.all_to_all(partial_proj, "ep", split_axis=0, concat_axis=2, tiled=True)
+    arrived = jnp.concatenate(
+        lax.all_to_all(jnp.stack(jnp.split(partial_proj, lax.axis_size("ep"), axis=0)), "ep", 0, 0),
+        axis=2,
+    )
     summed = lax.psum_scatter(arrived, "tp", scatter_dimension=2, tiled=True)
     projected = rounded(summed)
     new_state, heads_out = recurrence(

time: 207 us -> 221 us (1.068)
  local copies, waits for them, and re-layouts: 32.9 us -> 47.6 us
    unnamed x27 -> x54, local copies, waits for them, and re-layouts: 27.2 us -> 39 us
    another operation x1 -> x2, local copies, waits for them, and re-layouts: 0.98 us -> 3.91 us  [shards(): jnp.stack(jnp.split(partial_proj, lax.axis_size('ep'), axis=0))]
where the time goes in v1:
time: 221 us; the launch traced here: 220 us
  blocking collectives  69.1 us (31%)
  waiting for transfers between devices  49.1 us (22%)
  local copies, waits for them, and re-layouts  47.6 us (22%)
  matrix products  15.5 us (7%)
  between operations  14.5 us (7%)
  starting transfers between devices  12.9 us (6%)
  other arithmetic  11.5 us (5%)
    unnamed x54, local copies, waits for them, and re-layouts  39 us
    all_gather x1, blocking collectives, shards(): rows_piece = lax.all_gather(own_rows, 'ep', axis=0, tiled=True)  24.1 us
    all_gather x1, blocking collectives, shards(): lax.all_gather(heads_out, 'ep', axis=0, tiled=True)  22.5 us
    unnamed x3, waiting for transfers between devices  16 us
    all_to_all x1, blocking collectives, shards(): lax.all_to_all(buffer, 'ep', split_axis=0, concat_axis=0, tiled=True)  14.8 us
    all_to_all x1, waiting for transfers between devices, shards(): lax.all_to_all(jnp.stack(jnp.split(partial_proj, lax.axis_size('ep'), axi...  13.2 us
    reduce_scatter x1, waiting for transfers between devices, shards(): lax.psum_scatter(down_part.astype(jnp.bfloat16), 'tp', scatter_dimension=...  10.9 us
    dot_general x1, matrix products, recurrence(): jnp.einsum('shk,shkv->shv', query_act, state_next, precision=lax.Precisio...  8.88 us
  transfers between devices with their start and end apart: 5, of which 5 were waited for; matrix products, arithmetic and copies ran while one was open for 4% of the time, Pallas kernels for 0%

profile of v1, /device:TPU:0, one launch (start us, length us, event | category | flops | bytes accessed | tf_op | source)
XLA Modules:
  0.0 220.3 jit_solution(10295439069672509291)
XLA Ops:
  7.2 0.9 convert_element_type.76
  8.1 0.9 multiply_reduce_fusion.2
  9.0 0.8 dynamic-slice
  9.9 24.1 %all-gather = bf16[16,15,768]{2,1,0:T(8,128)(2,1)S(1)} all-gather(bf16[1,15,768]{2,1,0:T(8,128)(2,1)S(1)} %fusion.52), channel_id=1, replica_groups=mesh['ep'=16,'tp'=2] {'ep'}, dimensions={0}, use_global_device_ids=true | all-gather | bytes 391680 | tf_op jit(solution)/shard_map/all_gather | solution.py:67
  34.0 0.1 reshape.216
  34.2 1.2 convolution_bitcast_fusion.2
  35.3 1.2 convolution_bitcast_fusion.3
  36.5 1.2 convolution_bitcast_fusion.4
  37.7 0.3 convolution_bitcast_fusion.5
  38.0 0.7 fusion.32
  38.7 0.8 fusion.31
  39.5 0.8 fusion.30
  40.3 0.8 fusion.29
  41.1 0.8 fusion.28
  41.9 0.8 fusion.27
  42.7 0.8 fusion.26
  43.5 0.8 fusion.25
  44.3 0.8 fusion.24
  45.1 0.8 fusion.23
  45.8 0.8 fusion.22
  46.6 0.8 fusion.21
  47.4 0.8 fusion.20
  48.2 0.8 fusion.19
  49.0 0.8 fusion.18
  49.8 0.8 fusion.17
  50.6 3.1 %copy.64 = f32[16,15,4,96]{3,2,1,0:T(4,128)} copy(f32[16,15,4,96]{1,3,2,0:T(8,128)} %fusion.17) | data formatting | bytes 737280 | tf_op jit(solution)/shard_map/stack | solution.py:76
  53.7 3.6 %all-to-all-start = ((f32[16,15,4,96]{3,2,1,0:T(4,128)}), f32[16,15,4,96]{3,2,1,0:T(4,128)S(1)}, u32[]{:S(2)}, u32[]{:S(2)}) async-start(f32[16,15,4,96]{3,2,1,0:T(4,128)} %copy.64), calls=%async_computation | async-start | bytes 983040 | tf_op jit(solution)/shard_map/all_to_all | solution.py:76
  57.3 0.1 copy.69
  57.6 0.1 reduce_window_sum.11
  57.8 13.2 %all-to-all-done = f32[16,15,4,96]{3,2,1,0:T(4,128)S(1)} async-done(((f32[16,15,4,96]{3,2,1,0:T(4,128)}), f32[16,15,4,96]{3,2,1,0:T(4,128)S(1)}, u32[]{:S(2)}, u32[]{:S(2)}) %all-to-all-start) | async-done | bytes 368672 | tf_op jit(solution)/shard_map/all_to_all | solution.py:76
  71.0 7.4 %copy.79 = f32[15,4,16,96]{1,0,3,2:T(8,128)} copy(f32[15,4,16,96]{3,1,0,2:T(4,128)S(1)} %bitcast.159) | data formatting | bytes 737280
  78.4 9.6 %reshape.225 = f32[1536,60]{1,0:T(8,128)} reshape(f32[1536,15,4]{2,1,0:T(8,128)} %bitcast.157) | data formatting | bytes 737280
  88.0 0.2 select_reduce_fusion
  88.3 0.6 compare_and_fusion
  88.9 0.1 copy.71
  89.0 16.0 %reduce-scatter.7.cloned.1.call-done = f32[768,60]{1,0:T(8,128)} async-done(((f32[1536,60]{1,0:T(8,128)}), f32[768,60]{1,0:T(8,128)}) %reduce-scatter.7.cloned.1.call-update) | async-done | bytes 184336
  105.0 5.3 %reshape.226 = bf16[768,15,4]{2,1,0:T(8,128)(2,1)} reshape(f32[768,60]{1,0:T(8,128)} %reduce-scatter.7.cloned.1.call-done) | data formatting | bytes 276480
  110.2 4.4 %copy.78 = bf16[15,4,768]{2,1,0:T(4,128)(2,1)S(1)} copy(bf16[15,4,768]{1,0,2:T(8,128)(2,1)} %bitcast.158) | data formatting | bytes 184320
  114.7 0.6 slice_reduce_fusion
  115.4 8.9 %fusion.1 = f32[15,6,1,128]{3,2,1,0:T(1,128)S(1)} fusion(bf16[15,6,128,128]{3,2,1,0:T(8,128)(2,1)} %param.17, f32[15,6,128]{2,1,0:T(8,128)S(1)} %mul.167, f32[15,6,128]{2,1,0:T(8,128)S(1)} %get-tuple-element.8, f32[15,6,128]{2,1,0:T(8,128)S(1)} %get-tuple-element.9, f32[15,6,128,1]{2,1,0,3:T(8,128)S(1)} %multiply_bitcast_fusion), kind=kOutput, calls=%fused_computation.3 | convolution fusion | flops 23592960 | bytes 3179520 | tf_op jit(solution)/shard_map/shk,shkv->shv/dot_general | solution.py:31
  124.6 22.5 %all-gather.1 = bf16[16,15,768]{2,1,0:T(8,128)(2,1)S(1)} all-gather(bf16[1,15,768]{2,1,0:T(8,128)(2,1)S(1)} %reshape.217), channel_id=1, replica_groups=mesh['ep'=16,'tp'=2] {'ep'}, dimensions={0}, use_global_device_ids=true | all-gather | bytes 391680 | tf_op jit(solution)/shard_map/all_gather | solution.py:91
  147.1 0.1 reshape.218
  147.2 0.3 convolution_convert_fusion.2
  147.5 0.1 copy.66
  147.6 0.7 all_to_all.24
  148.3 3.6 %all-to-all-start.1 = ((bf16[16,15,96]{2,1,0:T(8,128)(2,1)}), bf16[16,15,96]{2,1,0:T(8,128)(2,1)S(1)}, u32[]{:S(2)}, u32[]{:S(2)}) async-start(bf16[16,15,96]{2,1,0:T(8,128)(2,1)} %all_to_all.24), calls=%async_computation.1 | async-start | bytes 131072 | tf_op jit(solution)/shard_map/all_to_all | solution.py:95
  152.1 6.7 %all-to-all-done.1 = bf16[16,15,96]{2,1,0:T(8,128)(2,1)S(1)} async-done(((bf16[16,15,96]{2,1,0:T(8,128)(2,1)}), bf16[16,15,96]{2,1,0:T(8,128)(2,1)S(1)}, u32[]{:S(2)}, u32[]{:S(2)}) %all-to-all-start.1) | async-done | bytes 46112 | tf_op jit(solution)/shard_map/all_to_all | solution.py:95
  158.8 0.1 all_to_all.27
  159.0 7.7 %psum.7 = bf16[15,1536]{1,0:T(8,128)(2,1)S(1)} all-reduce(bf16[15,1536]{1,0:T(8,128)(2,1)S(1)} %all_to_all.27), channel_id=1, replica_groups=mesh['ep'=16,'tp'=2] {'tp'}, use_global_device_ids=true, to_apply=%region_3.4 | all-reduce | flops 23040 | bytes 92160 | tf_op jit(solution)/shard_map/psum | solution.py:98
  166.7 0.1 multiply_reduce_fusion.1
  166.8 1.0 convolution_convert_fusion
  167.8 0.1 reshape.200
  167.9 14.8 %all_to_all.34 = bf16[16,6,1536]{2,1,0:T(8,128)(2,1)S(1)} all-to-all(bf16[16,6,1536]{2,1,0:T(8,128)(2,1)S(1)} %reshape.200), channel_id=1, replica_groups=mesh['ep'=16,'tp'=2] {'ep'}, dimensions={0} | all-to-all | bytes 589824 | tf_op jit(solution)/shard_map/all_to_all | solution.py:122
  182.7 0.3 convolution_bitcast_fusion.1
  183.0 1.4 fusion.5
  184.5 0.1 copy.68
  184.6 10.9 %reduce-scatter.5.cloned.1.call-done = bf16[16,1,6,768]{3,0,2,1:T(8,128)(2,1)} async-done(((bf16[16,1,6,1536]{3,0,2,1:T(8,128)(2,1)}), bf16[16,1,6,768]{3,0,2,1:T(8,128)(2,1)}) %reduce-scatter.5.cloned.1.call-update) | async-done | bytes 147472 | tf_op jit(solution)/shard_map/reduce_scatter | solution.py:133
  195.5 1.6 copy.74
  197.1 5.6 %all-to-all-start.3 = ((bf16[16,6,768]{2,1,0:T(8,128)(2,1)}), bf16[16,6,768]{2,1,0:T(8,128)(2,1)S(1)}, u32[]{:S(2)}, u32[]{:S(2)}) async-start(bf16[16,6,768]{2,1,0:T(8,128)(2,1)} %copy.74), calls=%async_computation.4 | async-start | bytes 393216 | tf_op jit(solution)/shard_map/all_to_all | solution.py:137
  202.8 6.7 %fusion = bf16[15,6,128,128]{3,2,1,0:T(8,128)(2,1)} fusion(bf16[15,6,128,128]{3,2,1,0:T(8,128)(2,1)} %param.17, f32[15,6,128]{2,1,0:T(8,128)S(1)} %mul.167, f32[15,6,128]{2,1,0:T(8,128)S(1)} %get-tuple-element.8, f32[15,6,128]{2,1,0:T(8,128)S(1)} %get-tuple-element.9), kind=kLoop, calls=%fused_computation.2 | loop fusion | flops 7372800 | bytes 6036480 | tf_op jit(solution)/shard_map/convert_element_type | solution.py:35
  209.5 2.3 %all-to-all-done.3 = bf16[16,6,768]{2,1,0:T(8,128)(2,1)S(1)} async-done(((bf16[16,6,768]{2,1,0:T(8,128)(2,1)}), bf16[16,6,768]{2,1,0:T(8,128)(2,1)S(1)}, u32[]{:S(2)}, u32[]{:S(2)}) %all-to-all-start.3) | async-done | bytes 147488 | tf_op jit(solution)/shard_map/all_to_all | solution.py:137
  211.8 0.8 gather_fusion
  212.6 0.2 multiply_reduce_fusion
  212.9 0.6 add_convert_fusion.1
  (64 shorter events, 1.2 us)
Async XLA Ops:
  7.2 175.8 %copy-start = (bf16[1,256,1536]{2,1,0:T(8,128)(2,1)S(1)}, bf16[1,256,1536]{2,1,0:T(8,128)(2,1)}, u32[]{:S(2)}) copy-start(bf16[1,256,1536]{2,1,0:T(8,128)(2,1)} %param.31) | copy-start | bytes 2359300
  7.2 30.5 %copy-start.4 = (bf16[768,96]{0,1:T(8,128)(2,1)S(1)}, bf16[768,96]{0,1:T(8,128)(2,1)}, u32[]{:S(2)}) copy-start(bf16[768,96]{0,1:T(8,128)(2,1)} %param.19) | copy-start | bytes 442372
  47.4 9.9 %copy-start.10 = (s32[15,6]{0,1:T(8,128)S(1)}, s32[15,6]{0,1:T(8,128)}, u32[]{:S(2)}) copy-start(s32[15,6]{0,1:T(8,128)} %param.27) | copy-start | bytes 1084
  53.7 17.3 %all-to-all-start = ((f32[16,15,4,96]{3,2,1,0:T(4,128)}), f32[16,15,4,96]{3,2,1,0:T(4,128)S(1)}, u32[]{:S(2)}, u32[]{:S(2)}) async-start(f32[16,15,4,96]{3,2,1,0:T(4,128)} %copy.64), calls=%async_computation | async-start | bytes 983040 | tf_op jit(solution)/shard_map/all_to_all | solution.py:76
  57.3 47.7 %reduce-scatter.7.cloned.1.call-start = ((), (), s32[]{:S(2)}) async-start(), calls=%async_computation.7 | async-start | bytes 1179648
  57.4 30.9 %copy-start.6 = (s32[15,6]{1,0:T(8,128)}, s32[15,6]{1,0:T(8,128)S(1)}, u32[]{:S(2)}) copy-start(s32[15,6]{1,0:T(8,128)S(1)} %copy.69) | copy-start | bytes 1084
  78.4 10.6 %copy-start.8 = (f32[768]{0:T(1024)S(1)}, f32[768]{0:T(1024)}, u32[]{:S(2)}) copy-start(f32[768]{0:T(1024)} %param.23) | copy-start | bytes 9220
  88.2 26.4 %copy-start.13 = (s32[90]{0:T(128)}, s32[90]{0:T(128)S(1)}, u32[]{:S(2)}) copy-start(s32[90]{0:T(128)S(1)} %select_reduce_fusion) | copy-start | bytes 1084
  115.3 9.1 %copy-start.12 = (f32[128]{0:T(128)S(1)}, f32[128]{0:T(128)}, u32[]{:S(2)}) copy-start(f32[128]{0:T(128)} %param.24) | copy-start | bytes 1540
  115.3 31.9 %copy-start.5 = (bf16[768,96]{0,1:T(8,128)(2,1)S(1)}, bf16[768,96]{0,1:T(8,128)(2,1)}, u32[]{:S(2)}) copy-start(bf16[768,96]{0,1:T(8,128)(2,1)} %param.25) | copy-start | bytes 442372
  115.4 51.3 %copy-start.3 = (bf16[15,1536]{1,0:T(8,128)(2,1)S(1)}, bf16[15,1536]{1,0:T(8,128)(2,1)}, u32[]{:S(2)}) copy-start(bf16[15,1536]{1,0:T(8,128)(2,1)} %param.16) | copy-start | bytes 138244
  124.3 58.4 %copy-start.1 = (bf16[1,1536,256]{2,1,0:T(8,128)(2,1)S(1)}, bf16[1,1536,256]{2,1,0:T(8,128)(2,1)}, u32[]{:S(2)}) copy-start(bf16[1,1536,256]{2,1,0:T(8,128)(2,1)} %param.29) | copy-start | bytes 2359300
  124.3 58.7 %copy-start.2 = (bf16[1,1536,256]{2,1,0:T(8,128)(2,1)S(1)}, bf16[1,1536,256]{2,1,0:T(8,128)(2,1)}, u32[]{:S(2)}) copy-start(bf16[1,1536,256]{2,1,0:T(8,128)(2,1)} %param.30) | copy-start | bytes 2359300
  148.3 36.1 %copy-start.7 = (s32[15,6]{1,0:T(8,128)S(1)}, s32[15,6]{1,0:T(8,128)}, u32[]{:S(2)}) copy-start(s32[15,6]{1,0:T(8,128)} %copy-done.6) | copy-start | bytes 1084
  148.3 36.2 %copy-start.11 = (f32[15,6]{0,1:T(8,128)S(1)}, f32[15,6]{0,1:T(8,128)}, u32[]{:S(2)}) copy-start(f32[15,6]{0,1:T(8,128)} %param.28) | copy-start | bytes 1084
  148.3 36.3 %copy-start.14 = (s32[90]{0:T(128)S(1)}, s32[90]{0:T(128)}, u32[]{:S(2)}) copy-start(s32[90]{0:T(128)} %copy-done.13) | copy-start | bytes 1084
  148.3 10.5 %all-to-all-start.1 = ((bf16[16,15,96]{2,1,0:T(8,128)(2,1)}), bf16[16,15,96]{2,1,0:T(8,128)(2,1)S(1)}, u32[]{:S(2)}, u32[]{:S(2)}) async-start(bf16[16,15,96]{2,1,0:T(8,128)(2,1)} %all_to_all.24), calls=%async_computation.1 | async-start | bytes 131072 | tf_op jit(solution)/shard_map/all_to_all | solution.py:95
  151.9 43.6 %reduce-scatter.5.cloned.1.call-start = ((), (), s32[]{:S(2)}) async-start(), calls=%async_computation.6 | async-start | bytes 442368 | tf_op jit(solution)/shard_map/reduce_scatter | solution.py:133
  197.1 14.6 %all-to-all-start.3 = ((bf16[16,6,768]{2,1,0:T(8,128)(2,1)}), bf16[16,6,768]{2,1,0:T(8,128)(2,1)S(1)}, u32[]{:S(2)}, u32[]{:S(2)}) async-start(bf16[16,6,768]{2,1,0:T(8,128)(2,1)} %copy.74), calls=%async_computation.4 | async-start | bytes 393216 | tf_op jit(solution)/shard_map/all_to_all | solution.py:137
  202.8 9.9 %copy-start.9 = (pred[15,6]{1,0:T(8,128)(4,1)S(1)}, pred[15,6]{1,0:T(8,128)(4,1)}, u32[]{:S(2)}) copy-start(pred[15,6]{1,0:T(8,128)(4,1)} %get-tuple-element.6) | copy-start | bytes 274
Sparse Core Ops, SparseCore 0:
  88.1 16.7 reduce-scatter.6
  184.5 10.9 reduce-scatter.4
